TPU v7x, 1024 devices: a whole 4x8x16 slice. The times are simulated.
1024 devices in a mesh: kv: 256 (over z, y, core), tp: 4 (over x).
Axes of the slice: x: 4, y: 8, z: 16, core: 2. Of those that a mesh axis runs over, the one named last changes fastest.
Arguments:
- queries: bfloat16 [65536, 4, 128], P('kv', 'tp'), may hold values from -6 to 6
- keys: bfloat16 [65536, 4, 128], P('kv', 'tp'), may hold values from -6 to 6
- values: bfloat16 [65536, 4, 128], P('kv', 'tp'), may hold values from -6 to 6
- attended: bfloat16 [65536, 4, 128], P('kv', 'tp'), may hold values from -6 to 6
- out_grad: bfloat16 [65536, 4, 128], P('kv', 'tp'), may hold values from -6 to 6
- log_sum: float32 [65536, 4], P('kv', 'tp'), may hold values from 2.5 to 4.5
- picked: int32 [512, 16], P('kv'), may hold values from -1 to 2047, as said below
- layer_input: bfloat16 [65536, 4096], P('kv'), may hold values from -0.09375 to 0.09375
Outputs:
- query_grad: float32 [65536, 4, 128], P('kv', 'tp')
- key_grad: float32 [65536, 4, 128], P('kv', 'tp')
- value_grad: float32 [65536, 4, 128], P('kv', 'tp')
- weight_grad: float32 [4096, 512], P('kv', 'tp')
Inputs may be any that keep to these rules, and one draw needn't show every extreme that they name: Row r lists distinct key block numbers picked by query block r, followed by -1 to the end of the row; at least one entry is not -1, and at most 16 are. No picked block starts after the last position of its query block. With the span of a position being the position divided by 256 (rounded down), the span of every picked block is the query block's span or that span less 1, 2, 4, 8 and so on. The query blocks of one span pick at most 4 distinct blocks from any other single span.
All inputs are finite; a program needn't handle non-finite values.
Results may differ from a plain program's by a relative error of at most 0.004.
Values may be sent and summed in bfloat16 or wider, within the bound.
A program may use at most 32 MiB of HBM per device.

v0:
```python
import jax
import jax.numpy as jnp
from jax import lax
from jax.sharding import Mesh
from jax.sharding import PartitionSpec as P

QB = 128
KB = 32
MAXSEL = 16
KV = ("kv_0", "kv_1", "kv_2")


def shifted(value, axis, by):
    count = lax.axis_size(axis)
    pairs = [(i, i + by) for i in range(count) if 0 <= i + by < count]
    return lax.ppermute(value, axis, pairs)


def reduced_to_own(parts, axes, sequence):
    inside = parts.shape[1:]
    parts = parts.reshape(*(lax.axis_size(a) for a in axes), *inside)
    parts = jnp.moveaxis(parts, sequence, range(len(axes))).reshape(-1, *inside)
    for k in sequence:
        parts = lax.psum_scatter(parts, axes[k], scatter_dimension=0, tiled=True)
    return parts[0]


def in_blocks(value, dim, count):
    before, after = (value.shape[:dim], value.shape[dim + 1 :])
    return jnp.moveaxis(value.reshape(*before, count, -1, *after), dim, 0)


def sum_by_axis(value, axes, sequence, dim):
    count = lax.axis_size(axes)
    return reduced_to_own(in_blocks(value, dim, count), axes, sequence)


def per_device(queries, keys, values, attended, out_grad, log_sum, picked, layer_input):
    tok_here, heads_here, head_dim = queries.shape
    query_count = tok_here // QB
    span_blocks = tok_here // KB
    key_slots = MAXSEL * KB
    levels = lax.axis_size(KV).bit_length() - 1
    device = lax.axis_index(KV)
    score_scale = head_dim ** (-0.5)
    row_dots = jnp.sum(out_grad.astype(jnp.float32) * attended.astype(jnp.float32), axis=-1)
    picked_live = picked >= 0
    safe_ids = jnp.where(picked_live, picked, 0)
    owner_span = safe_ids // span_blocks
    local_block = safe_ids % span_blocks
    powers = jnp.left_shift(jnp.ones((levels,), jnp.int32), jnp.arange(levels, dtype=jnp.int32))
    span_group = jnp.sum(((device - owner_span)[..., None] >= powers).astype(jnp.int32), axis=-1)
    key_parts = [keys]
    value_parts = [values]
    for level_bit in range(levels):
        got_keys, got_values = shifted((keys, values), KV, 1 << level_bit)
        key_parts.append(got_keys)
        value_parts.append(got_values)
    slot_base = span_group * tok_here + local_block * KB
    key_store = jnp.concatenate(key_parts, axis=0)
    value_store = jnp.concatenate(value_parts, axis=0)
    gather_rows = (slot_base[..., None] + jnp.arange(KB, dtype=jnp.int32)).reshape(
        query_count, key_slots
    )
    key_rows = key_store[gather_rows]
    value_rows = value_store[gather_rows]
    query_blocks = queries.reshape(query_count, QB, heads_here, head_dim)
    grad_blocks = out_grad.reshape(query_count, QB, heads_here, head_dim)
    query_pos = device * tok_here + jnp.arange(tok_here, dtype=jnp.int32).reshape(query_count, QB)
    key_pos = (safe_ids[..., None] * KB + jnp.arange(KB, dtype=jnp.int32)).reshape(
        query_count, key_slots
    )
    key_live = jnp.repeat(picked_live, KB, axis=1)
    pair_live = key_live[:, None, :] & (key_pos[:, None, :] <= query_pos[:, :, None])
    stored = log_sum.reshape(query_count, QB, heads_here).transpose(0, 2, 1)[..., None]
    block_dots = row_dots.reshape(query_count, QB, heads_here).transpose(0, 2, 1)[..., None]
    scores = (
        jnp.einsum("bqhd,bkhd->bhqk", query_blocks, key_rows, preferred_element_type=jnp.float32)
        * score_scale
    )
    weights = jnp.where(pair_live[:, None], jnp.exp(scores - stored), 0.0)
    slopes = jnp.einsum(
        "bqhd,bkhd->bhqk", grad_blocks, value_rows, preferred_element_type=jnp.float32
    )
    score_grad = weights * (slopes - block_dots)
    weight_pairs = weights.astype(jnp.bfloat16)
    grad_pairs = score_grad.astype(jnp.bfloat16)
    query_grad = (
        jnp.einsum("bhqk,bkhd->bqhd", grad_pairs, key_rows, preferred_element_type=jnp.float32)
        * score_scale
    )
    key_terms = (
        jnp.einsum("bhqk,bqhd->bkhd", grad_pairs, query_blocks, preferred_element_type=jnp.float32)
        * score_scale
    )
    value_terms = jnp.einsum(
        "bhqk,bqhd->bkhd", weight_pairs, grad_blocks, preferred_element_type=jnp.float32
    )
    store_rows = key_store.shape[0]
    flat_rows = gather_rows.reshape(-1)
    key_sums = (
        jnp.zeros((store_rows, heads_here, head_dim), jnp.float32)
        .at[flat_rows]
        .add(key_terms.reshape(-1, heads_here, head_dim))
    )
    value_sums = (
        jnp.zeros((store_rows, heads_here, head_dim), jnp.float32)
        .at[flat_rows]
        .add(value_terms.reshape(-1, heads_here, head_dim))
    )
    key_grad = key_sums[:tok_here]
    value_grad = value_sums[:tok_here]
    for level_bit in range(levels):
        first_row = (level_bit + 1) * tok_here
        back_keys, back_values = shifted(
            (
                key_sums[first_row : first_row + tok_here],
                value_sums[first_row : first_row + tok_here],
            ),
            KV,
            -(1 << level_bit),
        )
        key_grad = key_grad + back_keys
        value_grad = value_grad + back_values
    value_round = value_grad.astype(jnp.bfloat16).reshape(tok_here, heads_here * head_dim)
    weight_grad = sum_by_axis(
        lax.dot_general(
            layer_input, value_round, (((0,), (0,)), ((), ())), preferred_element_type=jnp.float32
        ),
        KV,
        (2, 0, 1),
        0,
    )
    return (query_grad.reshape(tok_here, heads_here, head_dim), key_grad, value_grad, weight_grad)


def solution(mesh):
    torus = Mesh(mesh.devices.reshape(16, 8, 2, mesh.shape["tp"]), ("kv_0", "kv_1", "kv_2", "tp"))
    return jax.shard_map(
        per_device,
        mesh=torus,
        in_specs=(
            P(KV, "tp", None),
            P(KV, "tp", None),
            P(KV, "tp", None),
            P(KV, "tp", None),
            P(KV, "tp", None),
            P(KV, "tp"),
            P(KV, None),
            P(KV, None),
        ),
        out_specs=(P(KV, "tp", None), P(KV, "tp", None), P(KV, "tp", None), P(KV, "tp")),
        check_vma=False,
    )
```

profile of v0, /device:TPU:1, one launch (start us, length us, event | category | flops | bytes accessed | tf_op | source)
XLA Modules:
  0.0 301.8 jit_solution(17048885873207334338)
XLA Ops:
  7.2 11.6 %collective-permute-start.6 = (bf16[256,1,128]{2,0,1:T(8,128)(2,1)}, bf16[256,1,128]{2,0,1:T(8,128)(2,1)S(1)}, u32[]{:S(2)}, u32[]{:S(2)}) collective-permute-start(bf16[256,1,128]{2,0,1:T(8,128)(2,1)} %param.9), channel_id=1, source_target_pairs={{0,256},{4,260},{8,264},{12,268},{16,272},{20,276},{24,280},{28,28... | collective-permute-start | bytes 196616 | tf_op jit(solution)/shard_map/ppermute | solution.py:16
  18.8 5.8 %collective-permute-start.5 = (bf16[256,1,128]{2,0,1:T(8,128)(2,1)}, bf16[256,1,128]{2,0,1:T(8,128)(2,1)S(1)}, u32[]{:S(2)}, u32[]{:S(2)}) collective-permute-start(bf16[256,1,128]{2,0,1:T(8,128)(2,1)} %param.9), channel_id=1, source_target_pairs={{0,128},{4,132},{8,136},{12,140},{16,144},{20,148},{24,152},{28,15... | collective-permute-start | bytes 196616 | tf_op jit(solution)/shard_map/ppermute | solution.py:16
  24.6 4.0 %collective-permute-start.4 = (bf16[256,1,128]{2,0,1:T(8,128)(2,1)}, bf16[256,1,128]{2,0,1:T(8,128)(2,1)S(1)}, u32[]{:S(2)}, u32[]{:S(2)}) collective-permute-start(bf16[256,1,128]{2,0,1:T(8,128)(2,1)} %param.9), channel_id=1, source_target_pairs={{0,64},{4,68},{8,72},{12,76},{16,80},{20,84},{24,88},{28,92},{32,9... | collective-permute-start | bytes 196616 | tf_op jit(solution)/shard_map/ppermute | solution.py:16
  28.6 7.5 %collective-permute-start.3 = (bf16[256,1,128]{2,0,1:T(8,128)(2,1)}, bf16[256,1,128]{2,0,1:T(8,128)(2,1)S(1)}, u32[]{:S(2)}, u32[]{:S(2)}) collective-permute-start(bf16[256,1,128]{2,0,1:T(8,128)(2,1)} %param.9), channel_id=1, source_target_pairs={{0,32},{4,36},{8,40},{12,44},{16,48},{20,52},{24,56},{28,60},{32,6... | collective-permute-start | bytes 196616 | tf_op jit(solution)/shard_map/ppermute | solution.py:16
  36.1 4.0 %collective-permute-start = (bf16[256,1,128]{2,0,1:T(8,128)(2,1)}, bf16[256,1,128]{2,0,1:T(8,128)(2,1)S(1)}, u32[]{:S(2)}, u32[]{:S(2)}) collective-permute-start(bf16[256,1,128]{2,0,1:T(8,128)(2,1)} %param.9), channel_id=1, source_target_pairs={{0,4},{4,8},{8,12},{12,16},{16,20},{20,24},{24,28},{28,32},{32,36}... | collective-permute-start | bytes 196616 | tf_op jit(solution)/shard_map/ppermute | solution.py:16
  44.0 2.3 collective-permute-start.1
  46.3 2.0 collective-permute-done.1
  48.3 4.1 %collective-permute-start.2 = (bf16[256,1,128]{2,0,1:T(8,128)(2,1)}, bf16[256,1,128]{2,0,1:T(8,128)(2,1)S(1)}, u32[]{:S(2)}, u32[]{:S(2)}) collective-permute-start(bf16[256,1,128]{2,0,1:T(8,128)(2,1)} %param.9), channel_id=1, source_target_pairs={{0,16},{4,20},{8,24},{12,28},{16,32},{20,36},{24,40},{28,44},{32,4... | collective-permute-start | bytes 196616 | tf_op jit(solution)/shard_map/ppermute | solution.py:16
  54.0 20.0 %collective-permute-start.7 = (bf16[256,1,128]{2,0,1:T(8,128)(2,1)}, bf16[256,1,128]{2,0,1:T(8,128)(2,1)S(1)}, u32[]{:S(2)}, u32[]{:S(2)}) collective-permute-start(bf16[256,1,128]{2,0,1:T(8,128)(2,1)} %param.9), channel_id=1, source_target_pairs={{0,512},{4,516},{8,520},{12,524},{16,528},{20,532},{24,536},{28,54... | collective-permute-start | bytes 196616 | tf_op jit(solution)/shard_map/ppermute | solution.py:16
  75.8 3.2 %gather_fusion = bf16[1024,128]{1,0:T(8,128)(2,1)S(1)} fusion(bf16[2304,128]{1,0:T(8,128)(2,1)S(1)} %bitcast.133, s32[1024]{0:T(1024)S(1)} %broadcast_clamp_fusion), kind=kCustom, calls=%fused_computation | custom fusion | bytes 528384 | tf_op jit(solution)/shard_map/gather | solution.py:65
  80.9 6.7 %scatter_custom_fusion.1 = f32[2304,128]{1,0:T(8,128)S(1)} fusion(s32[1024]{0:T(1024)S(1)} %bitcast.150, f32[1024,128]{1,0:T(8,128)} %bitcast.140, f32[]{:T(128)} %constant.71.clone.1), kind=kCustom, calls=%fused_computation.16 | custom fusion | flops 131072 | bytes 1180160 | tf_op jit(solution)/shard_map/scatter-add | solution.py:109
  94.2 9.8 %collective-permute-done.30 = f32[256,1,128]{2,0,1:T(8,128)S(1)} collective-permute-done((f32[256,1,128]{2,0,1:T(8,128)S(1)}, f32[256,1,128]{2,0,1:T(8,128)S(1)}, u32[]{:S(2)}, u32[]{:S(2)}) %collective-permute-start.30) | collective-permute-done | bytes 131104 | tf_op jit(solution)/shard_map/ppermute | solution.py:16
  105.3 5.5 %collective-permute-start.24 = (f32[256,1,128]{2,0,1:T(8,128)S(1)}, f32[256,1,128]{2,0,1:T(8,128)S(1)}, u32[]{:S(2)}, u32[]{:S(2)}) collective-permute-start(f32[256,1,128]{2,0,1:T(8,128)S(1)} %get-tuple-element.29), channel_id=1, source_target_pairs={{4,0},{8,4},{12,8},{16,12},{20,16},{24,20},{28,24},{32,28},{36,32}... | collective-permute-start | bytes 393224 | tf_op jit(solution)/shard_map/ppermute | solution.py:16
  112.2 3.5 %collective-permute-done.24 = f32[256,1,128]{2,0,1:T(8,128)S(1)} collective-permute-done((f32[256,1,128]{2,0,1:T(8,128)S(1)}, f32[256,1,128]{2,0,1:T(8,128)S(1)}, u32[]{:S(2)}, u32[]{:S(2)}) %collective-permute-start.24) | collective-permute-done | bytes 131104 | tf_op jit(solution)/shard_map/ppermute | solution.py:16
  115.8 11.7 %collective-permute-done.31 = f32[256,1,128]{2,1,0:T(1,128)S(1)} collective-permute-done((f32[256,1,128]{2,1,0:T(1,128)S(1)}, f32[256,1,128]{2,1,0:T(1,128)S(1)}, u32[]{:S(2)}, u32[]{:S(2)}) %collective-permute-start.31) | collective-permute-done | bytes 131104 | tf_op jit(solution)/shard_map/ppermute | solution.py:16
  130.2 2.9 copy.30
  133.1 3.2 %copy.31 = f32[2,16,8,16,128]{4,3,2,1,0:T(8,128)} copy(f32[2,16,8,16,128]{4,3,0,2,1:T(8,128)} %bitcast.132) | data formatting | bytes 4194304 | tf_op jit(solution)/shard_map/transpose | solution.py:22
  137.1 12.6 %collective-permute-start.14 = (bf16[256,1,128]{2,0,1:T(8,128)(2,1)S(1)}, bf16[256,1,128]{2,0,1:T(8,128)(2,1)S(1)}, u32[]{:S(2)}, u32[]{:S(2)}) collective-permute-start(bf16[256,1,128]{2,0,1:T(8,128)(2,1)S(1)} %copy-done.8), channel_id=1, source_target_pairs={{0,256},{4,260},{8,264},{12,268},{16,272},{20,276},{24,280},{28,28... | collective-permute-start | bytes 196616 | tf_op jit(solution)/shard_map/ppermute | solution.py:16
  149.8 6.8 %collective-permute-start.13 = (bf16[256,1,128]{2,0,1:T(8,128)(2,1)S(1)}, bf16[256,1,128]{2,0,1:T(8,128)(2,1)S(1)}, u32[]{:S(2)}, u32[]{:S(2)}) collective-permute-start(bf16[256,1,128]{2,0,1:T(8,128)(2,1)S(1)} %copy-done.8), channel_id=1, source_target_pairs={{0,128},{4,132},{8,136},{12,140},{16,144},{20,148},{24,152},{28,15... | collective-permute-start | bytes 196616 | tf_op jit(solution)/shard_map/ppermute | solution.py:16
  157.9 2.8 collective-permute-start.11
  160.7 4.8 %collective-permute-start.8 = (bf16[256,1,128]{2,0,1:T(8,128)(2,1)S(1)}, bf16[256,1,128]{2,0,1:T(8,128)(2,1)S(1)}, u32[]{:S(2)}, u32[]{:S(2)}) collective-permute-start(bf16[256,1,128]{2,0,1:T(8,128)(2,1)S(1)} %copy-done.8), channel_id=1, source_target_pairs={{0,4},{4,8},{8,12},{12,16},{16,20},{20,24},{24,28},{28,32},{32,36}... | collective-permute-start | bytes 196616 | tf_op jit(solution)/shard_map/ppermute | solution.py:16
  166.8 3.1 %collective-permute-start.9 = (bf16[256,1,128]{2,0,1:T(8,128)(2,1)S(1)}, bf16[256,1,128]{2,0,1:T(8,128)(2,1)S(1)}, u32[]{:S(2)}, u32[]{:S(2)}) collective-permute-start(bf16[256,1,128]{2,0,1:T(8,128)(2,1)S(1)} %copy-done.8), channel_id=1, source_target_pairs={{0,8},{4,12},{8,16},{12,20},{16,24},{20,28},{24,32},{28,36},{32,40... | collective-permute-start | bytes 196616 | tf_op jit(solution)/shard_map/ppermute | solution.py:16
  171.2 5.1 %collective-permute-start.10 = (bf16[256,1,128]{2,0,1:T(8,128)(2,1)S(1)}, bf16[256,1,128]{2,0,1:T(8,128)(2,1)S(1)}, u32[]{:S(2)}, u32[]{:S(2)}) collective-permute-start(bf16[256,1,128]{2,0,1:T(8,128)(2,1)S(1)} %copy-done.8), channel_id=1, source_target_pairs={{0,16},{4,20},{8,24},{12,28},{16,32},{20,36},{24,40},{28,44},{32,4... | collective-permute-start | bytes 196616 | tf_op jit(solution)/shard_map/ppermute | solution.py:16
  177.7 15.5 %collective-permute-start.15 = (bf16[256,1,128]{2,0,1:T(8,128)(2,1)S(1)}, bf16[256,1,128]{2,0,1:T(8,128)(2,1)S(1)}, u32[]{:S(2)}, u32[]{:S(2)}) collective-permute-start(bf16[256,1,128]{2,0,1:T(8,128)(2,1)S(1)} %copy-done.8), channel_id=1, source_target_pairs={{0,512},{4,516},{8,520},{12,524},{16,528},{20,532},{24,536},{28,54... | collective-permute-start | bytes 196616 | tf_op jit(solution)/shard_map/ppermute | solution.py:16
  194.5 4.3 %gather_fusion.1 = bf16[1024,128]{1,0:T(8,128)(2,1)} fusion(bf16[2304,128]{1,0:T(8,128)(2,1)S(1)} %bitcast.134, s32[1024]{0:T(1024)S(1)} %broadcast_clamp_fusion), kind=kCustom, calls=%fused_computation.1 | custom fusion | bytes 528384 | tf_op jit(solution)/shard_map/gather | solution.py:66
  201.8 6.7 %scatter_custom_fusion = f32[2304,128]{1,0:T(8,128)S(1)} fusion(s32[1024]{0:T(1024)S(1)} %bitcast.151, f32[1024,128]{1,0:T(8,128)} %bitcast.142, f32[]{:T(128)} %constant.71.clone.1), kind=kCustom, calls=%fused_computation.18 | custom fusion | flops 131072 | bytes 1180160 | tf_op jit(solution)/shard_map/scatter-add | solution.py:104
  209.3 5.5 %collective-permute-start.16 = (f32[256,1,128]{2,0,1:T(8,128)S(1)}, f32[256,1,128]{2,0,1:T(8,128)}, u32[]{:S(2)}, u32[]{:S(2)}) collective-permute-start(f32[256,1,128]{2,0,1:T(8,128)S(1)} %get-tuple-element.30), channel_id=1, source_target_pairs={{4,0},{8,4},{12,8},{16,12},{20,16},{24,20},{28,24},{32,28},{36,32}... | collective-permute-start | bytes 393224 | tf_op jit(solution)/shard_map/ppermute | solution.py:16
  221.3 13.7 %collective-permute-done.22 = f32[256,1,128]{2,0,1:T(8,128)} collective-permute-done((f32[256,1,128]{2,0,1:T(8,128)S(1)}, f32[256,1,128]{2,0,1:T(8,128)}, u32[]{:S(2)}, u32[]{:S(2)}) %collective-permute-start.22) | collective-permute-done | bytes 131104 | tf_op jit(solution)/shard_map/ppermute | solution.py:16
  238.6 2.7 reduce-scatter.6.cloned.1.call-done
  241.9 10.0 %collective-permute-done.23 = f32[256,1,128]{2,0,1:T(8,128)} collective-permute-done((f32[256,1,128]{2,0,1:T(8,128)}, f32[256,1,128]{2,0,1:T(8,128)}, u32[]{:S(2)}, u32[]{:S(2)}) %collective-permute-start.23) | collective-permute-done | bytes 131104 | tf_op jit(solution)/shard_map/ppermute | solution.py:16
  251.8 2.0 fusion.27
  253.8 41.4 %reduce-scatter.8.cloned.1.call-done = f32[1,16,128]{2,1,0:T(8,128)} async-done(((f32[8,16,128]{2,1,0:T(8,128)}), f32[1,16,128]{2,1,0:T(8,128)}) %reduce-scatter.8.cloned.1.call-update) | async-done | bytes 8208 | tf_op jit(solution)/shard_map/reduce_scatter | solution.py:24
  (120 shorter events, 42.4 us)
Async XLA Ops:
  7.2 158.5 %reduce-scatter.4.cloned.1.call-start = ((), (), s32[]{:S(2)}) async-start(), calls=%async_computation.3 | async-start | bytes 3145728 | tf_op jit(solution)/shard_map/reduce_scatter | solution.py:24
  7.2 67.0 %collective-permute-start.6 = (bf16[256,1,128]{2,0,1:T(8,128)(2,1)}, bf16[256,1,128]{2,0,1:T(8,128)(2,1)S(1)}, u32[]{:S(2)}, u32[]{:S(2)}) collective-permute-start(bf16[256,1,128]{2,0,1:T(8,128)(2,1)} %param.9), channel_id=1, source_target_pairs={{0,256},{4,260},{8,264},{12,268},{16,272},{20,276},{24,280},{28,28... | collective-permute-start | bytes 196616 | tf_op jit(solution)/shard_map/ppermute | solution.py:16
  18.8 55.4 %collective-permute-start.5 = (bf16[256,1,128]{2,0,1:T(8,128)(2,1)}, bf16[256,1,128]{2,0,1:T(8,128)(2,1)S(1)}, u32[]{:S(2)}, u32[]{:S(2)}) collective-permute-start(bf16[256,1,128]{2,0,1:T(8,128)(2,1)} %param.9), channel_id=1, source_target_pairs={{0,128},{4,132},{8,136},{12,140},{16,144},{20,148},{24,152},{28,15... | collective-permute-start | bytes 196616 | tf_op jit(solution)/shard_map/ppermute | solution.py:16
  24.6 49.5 %collective-permute-start.4 = (bf16[256,1,128]{2,0,1:T(8,128)(2,1)}, bf16[256,1,128]{2,0,1:T(8,128)(2,1)S(1)}, u32[]{:S(2)}, u32[]{:S(2)}) collective-permute-start(bf16[256,1,128]{2,0,1:T(8,128)(2,1)} %param.9), channel_id=1, source_target_pairs={{0,64},{4,68},{8,72},{12,76},{16,80},{20,84},{24,88},{28,92},{32,9... | collective-permute-start | bytes 196616 | tf_op jit(solution)/shard_map/ppermute | solution.py:16
  28.6 45.5 %collective-permute-start.3 = (bf16[256,1,128]{2,0,1:T(8,128)(2,1)}, bf16[256,1,128]{2,0,1:T(8,128)(2,1)S(1)}, u32[]{:S(2)}, u32[]{:S(2)}) collective-permute-start(bf16[256,1,128]{2,0,1:T(8,128)(2,1)} %param.9), channel_id=1, source_target_pairs={{0,32},{4,36},{8,40},{12,44},{16,48},{20,52},{24,56},{28,60},{32,6... | collective-permute-start | bytes 196616 | tf_op jit(solution)/shard_map/ppermute | solution.py:16
  36.1 7.8 %collective-permute-start = (bf16[256,1,128]{2,0,1:T(8,128)(2,1)}, bf16[256,1,128]{2,0,1:T(8,128)(2,1)S(1)}, u32[]{:S(2)}, u32[]{:S(2)}) collective-permute-start(bf16[256,1,128]{2,0,1:T(8,128)(2,1)} %param.9), channel_id=1, source_target_pairs={{0,4},{4,8},{8,12},{12,16},{16,20},{20,24},{24,28},{28,32},{32,36}... | collective-permute-start | bytes 196616 | tf_op jit(solution)/shard_map/ppermute | solution.py:16
  54.0 21.7 %collective-permute-start.7 = (bf16[256,1,128]{2,0,1:T(8,128)(2,1)}, bf16[256,1,128]{2,0,1:T(8,128)(2,1)S(1)}, u32[]{:S(2)}, u32[]{:S(2)}) collective-permute-start(bf16[256,1,128]{2,0,1:T(8,128)(2,1)} %param.9), channel_id=1, source_target_pairs={{0,512},{4,516},{8,520},{12,524},{16,528},{20,532},{24,536},{28,54... | collective-permute-start | bytes 196616 | tf_op jit(solution)/shard_map/ppermute | solution.py:16
  87.7 16.3 %collective-permute-start.30 = (f32[256,1,128]{2,0,1:T(8,128)S(1)}, f32[256,1,128]{2,0,1:T(8,128)S(1)}, u32[]{:S(2)}, u32[]{:S(2)}) collective-permute-start(f32[256,1,128]{2,0,1:T(8,128)S(1)} %get-tuple-element.23), channel_id=1, source_target_pairs={{256,0},{260,4},{264,8},{268,12},{272,16},{276,20},{280,24},{284,2... | collective-permute-start | bytes 393224 | tf_op jit(solution)/shard_map/ppermute | solution.py:16
  89.0 16.3 %collective-permute-start.29 = (f32[256,1,128]{2,0,1:T(8,128)S(1)}, f32[256,1,128]{2,0,1:T(8,128)S(1)}, u32[]{:S(2)}, u32[]{:S(2)}) collective-permute-start(f32[256,1,128]{2,0,1:T(8,128)S(1)} %get-tuple-element.24), channel_id=1, source_target_pairs={{128,0},{132,4},{136,8},{140,12},{144,16},{148,20},{152,24},{156,2... | collective-permute-start | bytes 393224 | tf_op jit(solution)/shard_map/ppermute | solution.py:16
  90.3 20.5 %collective-permute-start.28 = (f32[256,1,128]{2,0,1:T(8,128)S(1)}, f32[256,1,128]{2,0,1:T(8,128)S(1)}, u32[]{:S(2)}, u32[]{:S(2)}) collective-permute-start(f32[256,1,128]{2,0,1:T(8,128)S(1)} %get-tuple-element.25), channel_id=1, source_target_pairs={{64,0},{68,4},{72,8},{76,12},{80,16},{84,20},{88,24},{92,28},{96,3... | collective-permute-start | bytes 393224 | tf_op jit(solution)/shard_map/ppermute | solution.py:16
  91.6 20.5 %collective-permute-start.27 = (f32[256,1,128]{2,0,1:T(8,128)S(1)}, f32[256,1,128]{2,0,1:T(8,128)S(1)}, u32[]{:S(2)}, u32[]{:S(2)}) collective-permute-start(f32[256,1,128]{2,0,1:T(8,128)S(1)} %get-tuple-element.26), channel_id=1, source_target_pairs={{32,0},{36,4},{40,8},{44,12},{48,16},{52,20},{56,24},{60,28},{64,3... | collective-permute-start | bytes 393224 | tf_op jit(solution)/shard_map/ppermute | solution.py:16
  92.9 19.2 %collective-permute-start.26 = (f32[256,1,128]{2,0,1:T(8,128)S(1)}, f32[256,1,128]{2,0,1:T(8,128)S(1)}, u32[]{:S(2)}, u32[]{:S(2)}) collective-permute-start(f32[256,1,128]{2,0,1:T(8,128)S(1)} %get-tuple-element.27), channel_id=1, source_target_pairs={{16,0},{20,4},{24,8},{28,12},{32,16},{36,20},{40,24},{44,28},{48,3... | collective-permute-start | bytes 393224 | tf_op jit(solution)/shard_map/ppermute | solution.py:16
  104.0 8.1 %collective-permute-start.25 = (f32[256,1,128]{2,0,1:T(8,128)S(1)}, f32[256,1,128]{2,0,1:T(8,128)S(1)}, u32[]{:S(2)}, u32[]{:S(2)}) collective-permute-start(f32[256,1,128]{2,0,1:T(8,128)S(1)} %get-tuple-element.28), channel_id=1, source_target_pairs={{8,0},{12,4},{16,8},{20,12},{24,16},{28,20},{32,24},{36,28},{40,32... | collective-permute-start | bytes 393224 | tf_op jit(solution)/shard_map/ppermute | solution.py:16
  105.3 10.4 %collective-permute-start.24 = (f32[256,1,128]{2,0,1:T(8,128)S(1)}, f32[256,1,128]{2,0,1:T(8,128)S(1)}, u32[]{:S(2)}, u32[]{:S(2)}) collective-permute-start(f32[256,1,128]{2,0,1:T(8,128)S(1)} %get-tuple-element.29), channel_id=1, source_target_pairs={{4,0},{8,4},{12,8},{16,12},{20,16},{24,20},{28,24},{32,28},{36,32}... | collective-permute-start | bytes 393224 | tf_op jit(solution)/shard_map/ppermute | solution.py:16
  110.8 16.7 %collective-permute-start.31 = (f32[256,1,128]{2,1,0:T(1,128)S(1)}, f32[256,1,128]{2,1,0:T(1,128)S(1)}, u32[]{:S(2)}, u32[]{:S(2)}) collective-permute-start(f32[256,1,128]{2,1,0:T(1,128)S(1)} %bitcast.143), channel_id=1, source_target_pairs={{512,0},{516,4},{520,8},{524,12},{528,16},{532,20},{536,24},{540,2... | collective-permute-start | bytes 393224 | tf_op jit(solution)/shard_map/ppermute | solution.py:16
  136.3 105.0 %reduce-scatter.6.cloned.1.call-start = ((), (), s32[]{:S(2)}) async-start(), calls=%async_computation.4 | async-start | bytes 1114112 | tf_op jit(solution)/shard_map/reduce_scatter | solution.py:24
  137.1 56.1 %collective-permute-start.14 = (bf16[256,1,128]{2,0,1:T(8,128)(2,1)S(1)}, bf16[256,1,128]{2,0,1:T(8,128)(2,1)S(1)}, u32[]{:S(2)}, u32[]{:S(2)}) collective-permute-start(bf16[256,1,128]{2,0,1:T(8,128)(2,1)S(1)} %copy-done.8), channel_id=1, source_target_pairs={{0,256},{4,260},{8,264},{12,268},{16,272},{20,276},{24,280},{28,28... | collective-permute-start | bytes 196616 | tf_op jit(solution)/shard_map/ppermute | solution.py:16
  149.8 43.5 %collective-permute-start.13 = (bf16[256,1,128]{2,0,1:T(8,128)(2,1)S(1)}, bf16[256,1,128]{2,0,1:T(8,128)(2,1)S(1)}, u32[]{:S(2)}, u32[]{:S(2)}) collective-permute-start(bf16[256,1,128]{2,0,1:T(8,128)(2,1)S(1)} %copy-done.8), channel_id=1, source_target_pairs={{0,128},{4,132},{8,136},{12,140},{16,144},{20,148},{24,152},{28,15... | collective-permute-start | bytes 196616 | tf_op jit(solution)/shard_map/ppermute | solution.py:16
  156.6 36.6 %collective-permute-start.12 = (bf16[256,1,128]{2,0,1:T(8,128)(2,1)S(1)}, bf16[256,1,128]{2,0,1:T(8,128)(2,1)S(1)}, u32[]{:S(2)}, u32[]{:S(2)}) collective-permute-start(bf16[256,1,128]{2,0,1:T(8,128)(2,1)S(1)} %copy-done.8), channel_id=1, source_target_pairs={{0,64},{4,68},{8,72},{12,76},{16,80},{20,84},{24,88},{28,92},{32,9... | collective-permute-start | bytes 196616 | tf_op jit(solution)/shard_map/ppermute | solution.py:16
  157.9 35.3 %collective-permute-start.11 = (bf16[256,1,128]{2,0,1:T(8,128)(2,1)S(1)}, bf16[256,1,128]{2,0,1:T(8,128)(2,1)S(1)}, u32[]{:S(2)}, u32[]{:S(2)}) collective-permute-start(bf16[256,1,128]{2,0,1:T(8,128)(2,1)S(1)} %copy-done.8), channel_id=1, source_target_pairs={{0,32},{4,36},{8,40},{12,44},{16,48},{20,52},{24,56},{28,60},{32,6... | collective-permute-start | bytes 196616 | tf_op jit(solution)/shard_map/ppermute | solution.py:16
  160.7 6.1 %collective-permute-start.8 = (bf16[256,1,128]{2,0,1:T(8,128)(2,1)S(1)}, bf16[256,1,128]{2,0,1:T(8,128)(2,1)S(1)}, u32[]{:S(2)}, u32[]{:S(2)}) collective-permute-start(bf16[256,1,128]{2,0,1:T(8,128)(2,1)S(1)} %copy-done.8), channel_id=1, source_target_pairs={{0,4},{4,8},{8,12},{12,16},{16,20},{20,24},{24,28},{28,32},{32,36}... | collective-permute-start | bytes 196616 | tf_op jit(solution)/shard_map/ppermute | solution.py:16
  165.7 129.5 %reduce-scatter.8.cloned.1.call-start = ((), (), s32[]{:S(2)}) async-start(), calls=%async_computation.5 | async-start | bytes 73728 | tf_op jit(solution)/shard_map/reduce_scatter | solution.py:24
  171.2 6.4 %collective-permute-start.10 = (bf16[256,1,128]{2,0,1:T(8,128)(2,1)S(1)}, bf16[256,1,128]{2,0,1:T(8,128)(2,1)S(1)}, u32[]{:S(2)}, u32[]{:S(2)}) collective-permute-start(bf16[256,1,128]{2,0,1:T(8,128)(2,1)S(1)} %copy-done.8), channel_id=1, source_target_pairs={{0,16},{4,20},{8,24},{12,28},{16,32},{20,36},{24,40},{28,44},{32,4... | collective-permute-start | bytes 196616 | tf_op jit(solution)/shard_map/ppermute | solution.py:16
  177.7 16.8 %collective-permute-start.15 = (bf16[256,1,128]{2,0,1:T(8,128)(2,1)S(1)}, bf16[256,1,128]{2,0,1:T(8,128)(2,1)S(1)}, u32[]{:S(2)}, u32[]{:S(2)}) collective-permute-start(bf16[256,1,128]{2,0,1:T(8,128)(2,1)S(1)} %copy-done.8), channel_id=1, source_target_pairs={{0,512},{4,516},{8,520},{12,524},{16,528},{20,532},{24,536},{28,54... | collective-permute-start | bytes 196616 | tf_op jit(solution)/shard_map/ppermute | solution.py:16
  209.3 10.7 %collective-permute-start.16 = (f32[256,1,128]{2,0,1:T(8,128)S(1)}, f32[256,1,128]{2,0,1:T(8,128)}, u32[]{:S(2)}, u32[]{:S(2)}) collective-permute-start(f32[256,1,128]{2,0,1:T(8,128)S(1)} %get-tuple-element.30), channel_id=1, source_target_pairs={{4,0},{8,4},{12,8},{16,12},{20,16},{24,20},{28,24},{32,28},{36,32}... | collective-permute-start | bytes 393224 | tf_op jit(solution)/shard_map/ppermute | solution.py:16
  214.8 20.2 %collective-permute-start.22 = (f32[256,1,128]{2,0,1:T(8,128)S(1)}, f32[256,1,128]{2,0,1:T(8,128)}, u32[]{:S(2)}, u32[]{:S(2)}) collective-permute-start(f32[256,1,128]{2,0,1:T(8,128)S(1)} %get-tuple-element.31), channel_id=1, source_target_pairs={{256,0},{260,4},{264,8},{268,12},{272,16},{276,20},{280,24},{284,2... | collective-permute-start | bytes 393224 | tf_op jit(solution)/shard_map/ppermute | solution.py:16
  216.1 20.2 %collective-permute-start.21 = (f32[256,1,128]{2,0,1:T(8,128)S(1)}, f32[256,1,128]{2,0,1:T(8,128)}, u32[]{:S(2)}, u32[]{:S(2)}) collective-permute-start(f32[256,1,128]{2,0,1:T(8,128)S(1)} %get-tuple-element.32), channel_id=1, source_target_pairs={{128,0},{132,4},{136,8},{140,12},{144,16},{148,20},{152,24},{156,2... | collective-permute-start | bytes 393224 | tf_op jit(solution)/shard_map/ppermute | solution.py:16
  217.4 23.9 %collective-permute-start.20 = (f32[256,1,128]{2,0,1:T(8,128)}, f32[256,1,128]{2,0,1:T(8,128)}, u32[]{:S(2)}, u32[]{:S(2)}) collective-permute-start(f32[256,1,128]{2,0,1:T(8,128)} %get-tuple-element.33), channel_id=1, source_target_pairs={{64,0},{68,4},{72,8},{76,12},{80,16},{84,20},{88,24},{92,28},{96,3... | collective-permute-start | bytes 393224 | tf_op jit(solution)/shard_map/ppermute | solution.py:16
  218.7 22.6 %collective-permute-start.19 = (f32[256,1,128]{2,0,1:T(8,128)}, f32[256,1,128]{2,0,1:T(8,128)}, u32[]{:S(2)}, u32[]{:S(2)}) collective-permute-start(f32[256,1,128]{2,0,1:T(8,128)} %get-tuple-element.34), channel_id=1, source_target_pairs={{32,0},{36,4},{40,8},{44,12},{48,16},{52,20},{56,24},{60,28},{64,3... | collective-permute-start | bytes 393224 | tf_op jit(solution)/shard_map/ppermute | solution.py:16
  220.0 21.3 %collective-permute-start.18 = (f32[256,1,128]{2,0,1:T(8,128)}, f32[256,1,128]{2,0,1:T(8,128)}, u32[]{:S(2)}, u32[]{:S(2)}) collective-permute-start(f32[256,1,128]{2,0,1:T(8,128)} %get-tuple-element.35), channel_id=1, source_target_pairs={{16,0},{20,4},{24,8},{28,12},{32,16},{36,20},{40,24},{44,28},{48,3... | collective-permute-start | bytes 393224 | tf_op jit(solution)/shard_map/ppermute | solution.py:16
  235.0 6.9 %collective-permute-start.17 = (f32[256,1,128]{2,0,1:T(8,128)}, f32[256,1,128]{2,0,1:T(8,128)}, u32[]{:S(2)}, u32[]{:S(2)}) collective-permute-start(f32[256,1,128]{2,0,1:T(8,128)} %get-tuple-element.36), channel_id=1, source_target_pairs={{8,0},{12,4},{16,8},{20,12},{24,16},{28,20},{32,24},{36,28},{40,32... | collective-permute-start | bytes 393224 | tf_op jit(solution)/shard_map/ppermute | solution.py:16
  236.3 15.5 %collective-permute-start.23 = (f32[256,1,128]{2,0,1:T(8,128)}, f32[256,1,128]{2,0,1:T(8,128)}, u32[]{:S(2)}, u32[]{:S(2)}) collective-permute-start(f32[256,1,128]{2,0,1:T(8,128)} %get-tuple-element.37), channel_id=1, source_target_pairs={{512,0},{516,4},{520,8},{524,12},{528,16},{532,20},{536,24},{540,2... | collective-permute-start | bytes 393224 | tf_op jit(solution)/shard_map/ppermute | solution.py:16
  (14 other events, 214.1 us)
Sparse Core Ops, SparseCore 0:
  136.4 27.7 reduce-scatter.3
  167.6 73.6 reduce-scatter.5
  245.2 49.9 reduce-scatter.7
where the time goes:
time: 308 us; the launch traced here: 302 us
  starting transfers between devices  140 us (45%)
  waiting for transfers between devices  103 us (33%)
  other arithmetic  18.7 us (6%)
  local copies, waits for them, and re-layouts  17.4 us (6%)
  between operations  14.5 us (5%)
  matrix products  7.27 us (2%)
    ppermute x32, starting transfers between devices, shifted(): return lax.ppermute(value, axis, pairs)  140 us
    ppermute x32, waiting for transfers between devices, shifted(): return lax.ppermute(value, axis, pairs)  59.2 us
    reduce_scatter x3, waiting for transfers between devices, reduced_to_own(): parts = lax.psum_scatter(parts, axes[k], scatter_dimension=0, tiled=True)  44.2 us
    scatter-add x1, other arithmetic, per_device(): value_sums = jnp.zeros((store_rows, heads_here, head_dim), jnp.float32).a...  6.7 us
    scatter-add x1, other arithmetic, per_device(): key_sums = jnp.zeros((store_rows, heads_here, head_dim), jnp.float32).at[...  6.7 us
  transfers between devices with their start and end apart: 35, of which 15 were waited for; matrix products, arithmetic and copies ran while one was open for 7% of the time, Pallas kernels for 0%

commit v1 on v0

v1 whole, which is shorter than its diff:
```python
import jax
import jax.numpy as jnp
from jax import lax
from jax.experimental import pallas as pl
from jax.experimental.pallas import tpu as pltpu
from jax.sharding import PartitionSpec as P

MESH = pl.DeviceIdType.MESH
F32, BF16 = jnp.float32, jnp.bfloat16
NY, NZ = 8, 16
SPAN, DH, KB, D = 256, 128, 32, 4096
BLOCKS = SPAN // KB
SCALE = DH ** (-0.5)
DEAD = -1e30
YSTEP = {1: 1, 2: 2, 3: 4}
NT = (((1,), (1,)), ((), ()))
Y_ORDER = (4, 3, 5, 2, 6, 1, 7)
Z_ORDER = (8, 7, 9, 6, 10, 5, 11, 4, 12, 3, 13, 2, 14, 1, 15)


def dot(a, b):
    return jnp.dot(a, b, preferred_element_type=F32)


def main_kernel(
    picked_ref, q_hbm, k_hbm, v_hbm, o_hbm, g_hbm, ls_hbm, x_hbm,
    dq_ref, dk_ref, dv_ref, w_ref,
    qd_own, aux_own, kk, vv, oo, ls, kt, qd, aux, pbuf, sbuf, dqt, dq4,
    ret_out, ret_in, xx, xt, xr, vb, vm, pf, pb, yb, sf, sb, zb,
    lsem, qsend, qrecv, rsend, rrecv, xsem, vsem, ysend, yrecv, zsend, zrecv, late,
):
    me = lax.axis_index("kv")
    z, y, c = me // (2 * NY), (me // 2) % NY, me % 2

    def dev(zz, yy, cc):
        return zz * (2 * NY) + yy * 2 + cc

    mate = dev(z, y, 1 - c)
    cross = dev(z, (y + 7 + 2 * c) % NY, 1 - c)
    ypeer = {d: dev(z, (y + d) % NY, c) for d in range(1, NY)}
    zpeer = {d: dev((z + d) % NZ, y, c) for d in range(1, NZ)}
    partners = [mate, cross, *ypeer.values(), *zpeer.values()]
    beside_first = (me != 0) & ((me == 1) | (me == dev(0, NY - 1, 1)) | ((z == 0) & (c == 0)) | ((y == 0) & (c == 0)))

    def remote(src, dst, send, recv, target):
        return pltpu.make_async_remote_copy(
            src_ref=src, dst_ref=dst, send_sem=send, recv_sem=recv, device_id={"kv": target}, device_id_type=MESH
        )

    barrier = pltpu.get_barrier_semaphore()

    @pl.when(me != 0)
    def _():
        for p in partners:
            pl.semaphore_signal(barrier, inc=1, device_id={"kv": p}, device_id_type=MESH)

    loads = [
        pltpu.make_async_copy(q_hbm, qd_own.at[pl.ds(0, SPAN)], lsem.at[0]),
        pltpu.make_async_copy(g_hbm, qd_own.at[pl.ds(SPAN, SPAN)], lsem.at[1]),
        pltpu.make_async_copy(o_hbm, oo, lsem.at[2]),
        pltpu.make_async_copy(ls_hbm, ls, lsem.at[3]),
        pltpu.make_async_copy(k_hbm, kk, lsem.at[4]),
        pltpu.make_async_copy(v_hbm, vv, lsem.at[5]),
        pltpu.make_async_copy(x_hbm, xx, lsem.at[6]),
    ]
    for load in loads:
        load.start()

    picked = picked_ref[...]
    back = me - picked // BLOCKS
    group = jnp.zeros_like(picked)
    for level in range(8):
        group = group + (back >= (1 << level)).astype(jnp.int32)
    bit = (group - 1) * BLOCKS + picked % BLOCKS
    live = picked >= 0
    lane = lax.broadcasted_iota(jnp.int32, (1, SPAN), 1)

    def word_row(low, high):
        inside = live & (bit >= low) & (bit < high)
        value = jnp.where(inside, jnp.left_shift(jnp.ones_like(bit), jnp.where(inside, bit - low, 0)), 0)
        total = jnp.sum(value.astype(F32), axis=1, keepdims=True)
        return jnp.where(lane < SPAN // 2, total[0:1, :], total[1:2, :])

    own_word = word_row(-BLOCKS, 0)
    words = [word_row(0, 24), word_row(24, 48), word_row(48, 64)]
    for load in loads[:4]:
        load.wait()
    prod = qd_own[SPAN:, :].astype(F32) * oo[...].astype(F32)
    dots = jnp.sum(prod.T, axis=0, keepdims=True)
    aux_own[0:1, :] = ls[...]
    aux_own[1:2, :] = dots
    for i in range(3):
        aux_own[2 + i : 3 + i, :] = words[i]
    aux_own[5:8, :] = jnp.zeros((3, SPAN), F32)

    @pl.when(me == 0)
    def _():
        pl.semaphore_wait(barrier, len(partners))
        for p in partners:
            pl.semaphore_signal(late, inc=1, device_id={"kv": p}, device_id_type=MESH)

    @pl.when(me != 0)
    def _():
        pl.semaphore_wait(barrier, len(partners) - beside_first.astype(jnp.int32))

    def part(level, j, source, target):
        if j == 0:
            src = aux_own if source is None else aux.at[source]
            dst = aux.at[level]
        else:
            rows = pl.ds((j - 1) * SPAN, SPAN)
            src = qd_own.at[rows] if source is None else qd.at[source, rows]
            dst = qd.at[level, rows]
        return remote(src, dst, qsend.at[level, j], qrecv.at[level, j], target)

    def send(level, source, target):
        for j in range(3):
            part(level, j, source, target).start()

    down = {d: dev(z, (y + NY - d) % NY, c) for d in (1, 2, 4)}
    target = {0: jnp.where(c == 1, mate, cross), 4: dev(z - 1, y, c), 5: dev(z - 1, y, c), 6: dev(z - 2, y, c), 7: dev(z - 8, y, c)}
    owns = {0: (c == 1) | (y >= 1), 4: z >= 1, 7: z >= 8}
    sends = {0: owns[0] | (z < NZ - 1), 4: z >= 1, 5: (z >= 1) & (z < NZ - 1), 6: (z >= 2) & (z < NZ - 2), 7: z >= 8}
    origin = {0: jnp.where(c == 0, mate, cross), 4: dev(z + 1, y, c), 5: dev(z + 2, y, c), 6: dev(z + 4, y, c), 7: dev(z + 8, y, c)}
    gets = {0: (c == 0) | (y < NY - 1) | (z < NZ - 1), 4: z < NZ - 1, 5: z < NZ - 2, 6: z < NZ - 4, 7: z < NZ - 8}
    for level, d in YSTEP.items():
        target[level] = down[d]
        owns[level] = y >= d
        sends[level] = owns[level] | (z < NZ - 1)
        origin[level] = ypeer[d]
        gets[level] = (y + d < NY) | (z < NZ - 1)

    def begin(level, now):
        pl.when(owns[level] & now(target[level]))(lambda: send(level, None, target[level]))

    for level in (4, 7, 3, 2, 1, 0):
        begin(level, lambda t: t != 0)

    for load in loads[4:6]:
        load.wait()
    kt[...] = kk[...].T

    def attend(queries, grads, aux_view, row, shift, own):
        scores = lax.dot_general(kk[...], queries, NT, preferred_element_type=F32)
        slopes = lax.dot_general(vv[...], grads, NT, preferred_element_type=F32)
        info = aux_view[...]
        stored, block_dots = info[0:1, :], info[1:2, :]
        word = (own_word if own else info[row : row + 1, :]).astype(jnp.int32)
        for b in range(BLOCKS):
            rows = slice(b * KB, (b + 1) * KB)
            shifted = jnp.right_shift(word, shift + b)
            bias = jnp.where(shifted % 2 == 1, -stored, DEAD)
            weights = jnp.exp(scores[rows] * SCALE + bias)
            if own:
                key_at = b * KB + lax.broadcasted_iota(jnp.int32, (KB, SPAN), 0)
                query_at = lax.broadcasted_iota(jnp.int32, (KB, SPAN), 1)
                weights = jnp.where(key_at <= query_at, weights, 0.0)
            pbuf[rows, :] = weights.astype(BF16)
            sbuf[rows, :] = (weights * (slopes[rows] - block_dots)).astype(BF16)
        value_part = dot(pbuf[...], grads)
        key_part = dot(sbuf[...], queries)
        if own:
            dv_ref[...] = value_part
            dk_ref[...] = key_part
        else:
            dv_ref[...] += value_part
            dk_ref[...] += key_part
        return dot(kt[...], sbuf[...])

    dqt[...] = attend(qd_own[:SPAN, :], qd_own[SPAN:, :], aux_own, 0, 0, True)

    loads[6].wait()

    @pl.loop(0, NZ)
    def _(zz):
        cols = pl.ds(pl.multiple_of(zz * SPAN, SPAN), SPAN)
        turned = xx[:, cols].T
        place = pl.ds(pl.multiple_of(zz * 16, 16), 16)
        for yy in range(NY):
            for cc in range(2):
                xt[cc, yy, place, :] = turned[yy * 32 + cc * 16 : yy * 32 + cc * 16 + 16, :]

    x_copy = remote(xt.at[1 - c], xr, xsem.at[0], xsem.at[1], mate)
    pl.when(mate != 0)(x_copy.start)

    @pl.when(gets[4])
    def _():
        for j in range(3):
            part(4, j, None, target[4]).wait_recv()
            pl.when((z >= 1) & (target[5] != 0))(lambda: part(5, j, 4, target[5]).start())

    for level in (3, 2, 1, 0):
        pl.when(jnp.logical_not(owns[level]) & gets[4])(lambda: send(level, 4, target[level]))

    @pl.when(gets[5])
    def _():
        for j in range(3):
            part(5, j, None, target[5]).wait_recv()
            pl.when((z >= 2) & (target[6] != 0))(lambda: part(6, j, 5, target[6]).start())

    def give_back(level):
        return remote(ret_out.at[level], ret_in.at[level], rsend.at[level], rrecv.at[level], origin[level])

    def process(level, wait):
        if wait:
            for j in range(3):
                part(level, j, None, target[level]).wait_recv()
        got = attend(qd[level, :SPAN, :], qd[level, SPAN:, :], aux.at[level], 2 + level // 3, level % 3 * BLOCKS, False)
        if level == 4:
            dq4[...] = got
        else:
            ret_out[level] = got.astype(BF16)
            give_back(level).start()

    pl.when(gets[4])(lambda: process(4, False))
    for level in (0, 1, 2, 3):
        pl.when(gets[level])(lambda: process(level, True))

    @pl.when(beside_first)
    def _():
        pl.semaphore_wait(late, 1)
        for level in (4, 7, 3, 2, 1, 0):
            begin(level, lambda t: t == 0)
        pl.when(me == dev(1, 0, 0))(lambda: send(5, 4, 0))
        pl.when(me == dev(2, 0, 0))(lambda: send(6, 5, 0))
        pl.when(mate == 0)(x_copy.start)

    pl.when(gets[5])(lambda: process(5, False))
    for level in (6, 7):
        pl.when(gets[level])(lambda: process(level, True))

    vb[...] = dv_ref[...].astype(BF16)
    v_copy = remote(vb, vm, vsem.at[0], vsem.at[1], mate)
    v_copy.start()
    for d in range(NY):
        at = (y + d) % NY
        pf[d] = dot(xt[c, at], vb[...])
    x_copy.wait_recv()
    v_copy.wait_recv()

    def y_copy(d):
        return remote(pb.at[d], yb.at[d], ysend.at[d], yrecv.at[d], ypeer[d])

    for d in Y_ORDER:
        at = (y + d) % NY
        pb[d] = (pf[d] + dot(xr[at], vm[...])).astype(BF16)
        y_copy(d).start()
    total = pf[0] + dot(xr[y], vm[...])

    for level in (0, 1, 2, 3):
        @pl.when(sends[level])
        def _(level=level):
            give_back(level).wait_recv()

            @pl.when(owns[level])
            def _():
                dqt[...] += ret_in[level].astype(F32)

            @pl.when(jnp.logical_not(owns[level]))
            def _():
                dq4[...] += ret_in[level].astype(F32)

    @pl.when(gets[4])
    def _():
        ret_out[4] = dq4[...].astype(BF16)
        give_back(4).start()

    for d in Y_ORDER:
        y_copy(d).wait_recv()
        total = total + yb[d].astype(F32)
    for zz in range(NZ):
        rows = total[zz * 16 : zz * 16 + 16, :]
        sf[zz] = rows
        sb[zz] = rows.astype(BF16)

    def z_copy(d):
        return remote(sb.at[(z + d) % NZ], zb.at[d], zsend.at[d], zrecv.at[d], zpeer[d])

    for d in Z_ORDER:
        z_copy(d).start()

    for level, there in ((4, z >= 1), (5, z >= 2), (6, z >= 4), (7, z >= 8)):
        @pl.when(there)
        def _(level=level):
            give_back(level).wait_recv()
            dqt[...] += ret_in[level].astype(F32)

    dq_ref[...] = dqt[...].T

    out = sf[z]
    for d in Z_ORDER:
        z_copy(d).wait_recv()
        out = out + zb[d].astype(F32)
    w_ref[...] = out

    for level in range(8):
        @pl.when(sends[level])
        def _(level=level):
            for j in range(3):
                part(level, j, None, target[level]).wait_send()

        pl.when(gets[level])(give_back(level).wait_send)
    x_copy.wait_send()
    v_copy.wait_send()
    for d in Y_ORDER:
        y_copy(d).wait_send()
    for d in Z_ORDER:
        z_copy(d).wait_send()


def last_kernel(dq_in, dk_in, dv_in, w_in, dq_ref, dk_ref, dv_ref, w_ref):
    dq_ref[...] = dq_in[...] * SCALE
    dk_ref[...] = dk_in[...] * SCALE
    dv_ref[...] = dv_in[...]
    w_ref[...] = w_in[...]


def per_device(queries, keys, values, attended, out_grad, log_sum, picked, layer_input):
    flat = [a.reshape(SPAN, DH) for a in (queries, keys, values, attended, out_grad)]
    stored = log_sum.reshape(1, SPAN)
    hbm = pl.BlockSpec(memory_space=pl.ANY)
    vmem = pl.BlockSpec(memory_space=pltpu.VMEM)
    outs = [jax.ShapeDtypeStruct((SPAN, DH), F32)] * 3 + [jax.ShapeDtypeStruct((16, DH), F32)]
    sem = pltpu.SemaphoreType.DMA
    scratch = [
        pltpu.VMEM((2 * SPAN, DH), BF16),
        pltpu.VMEM((8, SPAN), F32),
        pltpu.VMEM((SPAN, DH), BF16),
        pltpu.VMEM((SPAN, DH), BF16),
        pltpu.VMEM((SPAN, DH), BF16),
        pltpu.VMEM((1, SPAN), F32),
        pltpu.VMEM((DH, SPAN), BF16),
        pltpu.VMEM((8, 2 * SPAN, DH), BF16),
        pltpu.VMEM((8, 8, SPAN), F32),
        pltpu.VMEM((SPAN, SPAN), BF16),
        pltpu.VMEM((SPAN, SPAN), BF16),
        pltpu.VMEM((DH, SPAN), F32),
        pltpu.VMEM((DH, SPAN), F32),
        pltpu.VMEM((8, DH, SPAN), BF16),
        pltpu.VMEM((8, DH, SPAN), BF16),
        pltpu.VMEM((SPAN, D), BF16),
        pltpu.VMEM((2, NY, SPAN, SPAN), BF16),
        pltpu.VMEM((NY, SPAN, SPAN), BF16),
        pltpu.VMEM((SPAN, DH), BF16),
        pltpu.VMEM((SPAN, DH), BF16),
        pltpu.VMEM((NY, SPAN, DH), F32),
        pltpu.VMEM((NY, SPAN, DH), BF16),
        pltpu.VMEM((NY, SPAN, DH), BF16),
        pltpu.VMEM((NZ, 16, DH), F32),
        pltpu.VMEM((NZ, 16, DH), BF16),
        pltpu.VMEM((NZ, 16, DH), BF16),
        sem((7,)), sem((8, 3)), sem((8, 3)), sem((8,)), sem((8,)), sem((2,)), sem((2,)),
        sem((NY,)), sem((NY,)), sem((NZ,)), sem((NZ,)), pltpu.SemaphoreType.REGULAR,
    ]
    got = pl.pallas_call(
        main_kernel,
        out_shape=outs,
        in_specs=[vmem] + [hbm] * 7,
        out_specs=[vmem] * 4,
        scratch_shapes=scratch,
        compiler_params=pltpu.CompilerParams(collective_id=0, has_side_effects=True),
        name="exchange",
    )(picked, *flat, stored, layer_input)
    got = pl.pallas_call(last_kernel, out_shape=outs, in_specs=[vmem] * 4, out_specs=[vmem] * 4, name="finish")(*got)
    return tuple(a.reshape(SPAN, 1, DH) for a in got[:3]) + (got[3],)


def solution(mesh):
    return jax.shard_map(
        per_device,
        mesh=mesh,
        in_specs=(P("kv", "tp", None),) * 5 + (P("kv", "tp"), P("kv", None), P("kv", None)),
        out_specs=(P("kv", "tp", None),) * 3 + (P("kv", "tp"),),
        check_vma=False,
    )
```

time: 308 us -> 82.9 us (0.27); the launches traced: 302 us -> 82 us
  starting transfers between devices: 140 us -> 0 us
  waiting for transfers between devices: 103 us -> 0 us
  Pallas kernels: 0 us -> 81.3 us
  other arithmetic: 18.7 us -> 0 us
  local copies, waits for them, and re-layouts: 17.4 us -> 0 us
  between operations: 14.5 us -> 0.64 us
  matrix products: 7.27 us -> 0 us
    ppermute x32 -> x0, starting transfers between devices: 140 us -> none  [shifted(): return lax.ppermute(value, axis, pairs)]
    pallas_call x0 -> x2, Pallas kernels: none -> 81.3 us  [the longest x1 79.5 us: per_device(): pl.pallas_call(main_kernel, out_shape=outs, in_specs=[vmem] + [hbm] * 7,...]
    ppermute x32 -> x0, waiting for transfers between devices: 59.2 us -> none  [shifted(): return lax.ppermute(value, axis, pairs)]
    reduce_scatter x3 -> x0, waiting for transfers between devices: 44.2 us -> none  [reduced_to_own(): parts = lax.psum_scatter(parts, axes[k], scatter_dimension=0, tiled=True)]
    scatter-add x2 -> x0, other arithmetic: 13.4 us -> none  [the longest x1 6.7 us: per_device(): value_sums = jnp.zeros((store_rows, heads_here, head_dim), jnp.float32).a...]
    gather x2 -> x0, local copies, waits for them, and re-layouts: 7.47 us -> none  [the longest x1 4.26 us: per_device(): value_rows = value_store[gather_rows]]
    dot_general x6 -> x0, matrix products: 7.27 us -> none  [the longest x1 1.84 us: per_device(): jnp.einsum('bhqk,bqhd->bkhd', grad_pairs, query_blocks, preferred_element...]
    transpose x1 -> x0, local copies, waits for them, and re-layouts: 3.21 us -> none  [reduced_to_own(): parts = jnp.moveaxis(parts, sequence, range(len(axes))).reshape(-1, *inside)]
  transfers between devices with their start and end apart: 35 -> 0, of which waited for: 15 -> 0; matrix products, arithmetic and copies ran while one was open for 7% -> 0% of each run, Pallas kernels for 0% -> 0%
where the time goes in v1:
time: 82.9 us; the launch traced here: 82 us
  Pallas kernels  81.3 us (98%)
    pallas_call x1, Pallas kernels, per_device(): pl.pallas_call(main_kernel, out_shape=outs, in_specs=[vmem] + [hbm] * 7,...  79.5 us
    pallas_call x1, Pallas kernels, per_device(): pl.pallas_call(last_kernel, out_shape=outs, in_specs=[vmem] * 4, out_spec...  1.79 us

profile of v1, /device:TPU:1, one launch (start us, length us, event | category | flops | bytes accessed | tf_op | source)
XLA Modules:
  0.0 82.0 jit_solution(2690071275426615540)
XLA Ops:
  0.6 79.5 %exchange.1 = (f32[256,128]{1,0:T(8,128)}, f32[256,128]{1,0:T(8,128)}, f32[256,128]{1,0:T(8,128)}, f32[16,128]{1,0:T(8,128)}) custom-call(s32[2,16]{1,0:T(2,128)} %picked_ref.1, bf16[256,128]{1,0:T(8,128)(2,1)} %bitcast.15, bf16[256,128]{1,0:T(8,128)(2,1)} %bitcast.16, bf16[256,128]{1,0:T(8,128)(2,1)} %bitcast.17, bf16[256,128]{1,0:T(8,128)(2,1)} %bitcast.18, ...), custom_call_target="tpu_custom_call" | custom-call | tf_op jit(solution)/shard_map/exchange/pallas_call | solution.py:355
  80.2 1.8 %finish.1 = (f32[256,128]{1,0:T(8,128)}, f32[256,128]{1,0:T(8,128)}, f32[256,128]{1,0:T(8,128)}, f32[16,128]{1,0:T(8,128)}) custom-call(f32[256,128]{1,0:T(8,128)} %get-tuple-element.12.dq_in, f32[256,128]{1,0:T(8,128)} %get-tuple-element.13.dk_in, f32[256,128]{1,0:T(8,128)} %get-tuple-element.14.dv_in, f32[16,128]{1,0:T(8,128)} %get-tuple-element.15.w_in), custom_call_target="tpu_custom_call" | custom-call | tf_op jit(solution)/shard_map/finish/pallas_call | solution.py:364
